TPU v7x, 512 devices: a whole 4x8x8 slice. The times are simulated.
512 devices in a mesh: sp: 256 (over z, y, x), tp: 2 (over core).
Axes of the slice: x: 4, y: 8, z: 8, core: 2. Of those that a mesh axis runs over, the one named last changes fastest.
Arguments:
- queries: bfloat16 [131072, 8, 128], P('sp', 'tp'), may hold values from -60 to 60
- keys: bfloat16 [131072, 8, 128], P('sp', 'tp'), may hold values from -40 to 40
- values: bfloat16 [131072, 8, 128], P('sp', 'tp'), may hold values from -6 to 6
- w_out: bfloat16 [1024, 2048], P(None, 'tp'), may hold values from -0.1875 to 0.1875
Outputs:
- mixed: bfloat16 [131072, 2048], P('sp', 'tp')
All inputs are finite; a program needn't handle non-finite values.
Results may differ from a plain program's by a relative error of at most 0.0051.
Values may be sent and summed in bfloat16 or wider, within the bound.
No kernel may reach another device: no remote copies, remote signals or barrier semaphores. Data moves between devices by JAX's collectives and lax.ppermute only.
A program may use at most 64 MiB of HBM per device.

v0:
```python
import math

import jax
import jax.numpy as jnp
from jax import lax
from jax.sharding import PartitionSpec as P

W1 = 128
WINDOW_TWO = 512
DILATION_TWO = 4
WINDOW_THREE = 2048
DILATION_THREE = 16


def from_behind(block, axis, distance):
    devices = range(lax.axis_size(axis))
    route = [(i - distance, i) for i in devices if i - distance in devices]
    return lax.ppermute(block, axis, route)


def sent_to_all(array, axis):
    peers = lax.axis_size(axis)
    return lax.all_to_all(
        jnp.broadcast_to(array[None], (peers, *array.shape)), axis, 0, 0, tiled=True
    )


def joined_along(parts, dim):
    shape = list(parts.shape[1:])
    shape[dim] *= parts.shape[0]
    return jnp.moveaxis(parts, 0, dim).reshape(shape)


def gather_directly(array, axis, dim):
    parts = sent_to_all(array, axis)
    return joined_along(parts, dim)


def branch_attend(queries, key_holder, value_holder, leading_total, leading_row, window, dilation):
    tok_rows, head_local, head_dim = queries.shape
    band_rows = window // dilation
    query_rows = tok_rows // dilation
    lead_rows = leading_total // dilation
    query_res = queries.reshape(query_rows, dilation, head_local, head_dim)
    key_res = key_holder.reshape(-1, dilation, head_local, head_dim)[
        lead_rows - band_rows : lead_rows + query_rows
    ]
    value_res = value_holder.reshape(-1, dilation, head_local, head_dim)[
        lead_rows - band_rows : lead_rows + query_rows
    ]
    scores = jnp.einsum(
        "qrhd,krhd->rhqk", query_res, key_res, preferred_element_type=jnp.float32
    ) / math.sqrt(head_dim)
    query_idx = jnp.arange(query_rows, dtype=jnp.int32)[:, None]
    key_idx = jnp.arange(query_rows + band_rows, dtype=jnp.int32)[None, :]
    distance = query_idx + band_rows - key_idx
    allowed = (
        (distance >= 0)
        & (distance <= band_rows)
        & (leading_row // dilation + key_idx - band_rows >= 0)
    )
    scores = jnp.where(allowed[None, None], scores, -jnp.inf)
    row_max = jnp.max(scores, axis=-1, keepdims=True)
    numerators = jnp.exp(scores - row_max)
    row_sum = jnp.sum(numerators, axis=-1, keepdims=True)
    weighted = jnp.einsum(
        "rhqk,krhd->qrhd",
        numerators.astype(jnp.bfloat16),
        value_res,
        preferred_element_type=jnp.float32,
    )
    branch_out = (weighted / jnp.transpose(row_sum, (2, 0, 1, 3))).reshape(
        tok_rows, head_local, head_dim
    )
    log_total = jnp.transpose((row_max + jnp.log(row_sum))[..., 0], (2, 0, 1)).reshape(
        tok_rows, head_local
    )
    return (branch_out, log_total)


def local(queries, keys, values, w_out):
    tok_rows, head_local, head_dim = queries.shape
    reach_pieces = WINDOW_THREE // tok_rows
    earlier_keys = []
    earlier_values = []
    for distance in range(reach_pieces, 0, -1):
        moved_keys, moved_values = from_behind((keys, values), "sp", distance)
        earlier_keys.append(moved_keys)
        earlier_values.append(moved_values)
    key_holder = jnp.concatenate(earlier_keys + [keys], axis=0)
    value_holder = jnp.concatenate(earlier_values + [values], axis=0)
    leading_row = lax.axis_index("sp") * tok_rows
    leading_total = reach_pieces * tok_rows
    first_out, first_total = branch_attend(
        queries, key_holder, value_holder, leading_total, leading_row, W1, 1
    )
    second_output, second_branch_total = branch_attend(
        queries, key_holder, value_holder, leading_total, leading_row, WINDOW_TWO, DILATION_TWO
    )
    third_output, third_branch_total = branch_attend(
        queries, key_holder, value_holder, leading_total, leading_row, WINDOW_THREE, DILATION_THREE
    )
    weights = jax.nn.softmax(
        jnp.stack([first_total, second_branch_total, third_branch_total]), axis=0
    )
    combined = jnp.sum(
        weights[..., None] * jnp.stack([first_out, second_output, third_output]), axis=0
    )
    attended = combined.reshape(tok_rows, head_local * head_dim).astype(jnp.bfloat16)
    projected = jnp.dot(
        gather_directly(attended, "tp", 1), w_out, preferred_element_type=jnp.float32
    )
    return projected.astype(jnp.bfloat16)


def solution(mesh):
    in_specs = (P("sp", "tp", None), P("sp", "tp", None), P("sp", "tp", None), P(None, "tp"))
    out_specs = P("sp", "tp")
    return jax.shard_map(local, mesh=mesh, in_specs=in_specs, out_specs=out_specs, check_vma=False)
```

profile of v0, /device:TPU:257, one launch (start us, length us, event | category | flops | bytes accessed | tf_op | source)
XLA Modules:
  0.0 142.9 jit_solution(2854478459420060616)
XLA Ops:
  0.0 2.1 %copy.63 = bf16[512,4,128]{2,0,1:T(8,128)(2,1)} copy(bf16[512,4,128]{2,1,0:T(4,128)(2,1)} %param.5) | data formatting | bytes 1048576 | tf_op args[1]
  2.1 3.1 %collective-permute-start = (bf16[512,4,128]{2,0,1:T(8,128)(2,1)}, bf16[512,4,128]{2,0,1:T(8,128)(2,1)}, u32[]{:S(2)}, u32[]{:S(2)}) collective-permute-start(bf16[512,4,128]{2,0,1:T(8,128)(2,1)} %copy.63), channel_id=1, source_target_pairs={{0,2},{2,4},{4,6},{6,8},{8,10},{10,12},{12,14},{14,16},{16,18},{18... | collective-permute-start | bytes 1572872 | tf_op jit(solution)/shard_map/ppermute | solution.py:18
  5.2 3.2 %collective-permute-start.1 = (bf16[512,4,128]{2,0,1:T(8,128)(2,1)}, bf16[512,4,128]{2,0,1:T(8,128)(2,1)}, u32[]{:S(2)}, u32[]{:S(2)}) collective-permute-start(bf16[512,4,128]{2,0,1:T(8,128)(2,1)} %copy.63), channel_id=1, source_target_pairs={{0,8},{2,10},{4,12},{6,14},{8,16},{10,18},{12,20},{14,22},{16,24},... | collective-permute-start | bytes 1572872 | tf_op jit(solution)/shard_map/ppermute | solution.py:18
  8.4 4.4 %collective-permute-start.2 = (bf16[512,4,128]{2,0,1:T(8,128)(2,1)}, bf16[512,4,128]{2,0,1:T(8,128)(2,1)}, u32[]{:S(2)}, u32[]{:S(2)}) collective-permute-start(bf16[512,4,128]{2,0,1:T(8,128)(2,1)} %copy.63), channel_id=1, source_target_pairs={{0,6},{2,8},{4,10},{6,12},{8,14},{10,16},{12,18},{14,20},{16,22},{... | collective-permute-start | bytes 1572872 | tf_op jit(solution)/shard_map/ppermute | solution.py:18
  12.8 3.4 %collective-permute-start.3 = (bf16[512,4,128]{2,0,1:T(8,128)(2,1)}, bf16[512,4,128]{2,0,1:T(8,128)(2,1)}, u32[]{:S(2)}, u32[]{:S(2)}) collective-permute-start(bf16[512,4,128]{2,0,1:T(8,128)(2,1)} %copy.63), channel_id=1, source_target_pairs={{0,4},{2,6},{4,8},{6,10},{8,12},{10,14},{12,16},{14,18},{16,20},{1... | collective-permute-start | bytes 1572872 | tf_op jit(solution)/shard_map/ppermute | solution.py:18
  16.2 1.3 copy.78
  17.6 3.3 %collective-permute-start.5 = (bf16[512,4,128]{0,2,1:T(8,128)(2,1)S(1)}, bf16[512,4,128]{0,2,1:T(8,128)(2,1)}, u32[]{:S(2)}, u32[]{:S(2)}) collective-permute-start(bf16[512,4,128]{0,2,1:T(8,128)(2,1)S(1)} %copy.78), channel_id=1, source_target_pairs={{0,8},{2,10},{4,12},{6,14},{8,16},{10,18},{12,20},{14,22},{16,24},... | collective-permute-start | bytes 1572872 | tf_op jit(solution)/shard_map/ppermute | solution.py:18
  21.0 0.4 fusion.30
  21.4 0.1 fusion.52
  21.6 1.6 %collective-permute-done.1 = bf16[512,4,128]{2,0,1:T(8,128)(2,1)} collective-permute-done((bf16[512,4,128]{2,0,1:T(8,128)(2,1)}, bf16[512,4,128]{2,0,1:T(8,128)(2,1)}, u32[]{:S(2)}, u32[]{:S(2)}) %collective-permute-start.1) | collective-permute-done | bytes 524320 | tf_op jit(solution)/shard_map/ppermute | solution.py:18
  23.2 12.7 %collective-permute-start.6 = (bf16[512,4,128]{0,2,1:T(8,128)(2,1)S(1)}, bf16[512,4,128]{0,2,1:T(8,128)(2,1)}, u32[]{:S(2)}, u32[]{:S(2)}) collective-permute-start(bf16[512,4,128]{0,2,1:T(8,128)(2,1)S(1)} %copy.78), channel_id=1, source_target_pairs={{0,6},{2,8},{4,10},{6,12},{8,14},{10,16},{12,18},{14,20},{16,22},{... | collective-permute-start | bytes 1572872 | tf_op jit(solution)/shard_map/ppermute | solution.py:18
  35.9 1.1 constant_dynamic-update-slice_fusion.6
  37.0 11.0 %collective-permute-start.7 = (bf16[512,4,128]{0,2,1:T(8,128)(2,1)S(1)}, bf16[512,4,128]{0,2,1:T(8,128)(2,1)}, u32[]{:S(2)}, u32[]{:S(2)}) collective-permute-start(bf16[512,4,128]{0,2,1:T(8,128)(2,1)S(1)} %copy.78), channel_id=1, source_target_pairs={{0,4},{2,6},{4,8},{6,10},{8,12},{10,14},{12,16},{14,18},{16,20},{1... | collective-permute-start | bytes 1572872 | tf_op jit(solution)/shard_map/ppermute | solution.py:18
  48.1 1.1 constant_dynamic-update-slice_fusion.5
  49.2 9.5 %collective-permute-start.4 = (bf16[512,4,128]{0,2,1:T(8,128)(2,1)S(1)}, bf16[512,4,128]{0,2,1:T(8,128)(2,1)}, u32[]{:S(2)}, u32[]{:S(2)}) collective-permute-start(bf16[512,4,128]{0,2,1:T(8,128)(2,1)S(1)} %copy.78), channel_id=1, source_target_pairs={{0,2},{2,4},{4,6},{6,8},{8,10},{10,12},{12,14},{14,16},{16,18},{18... | collective-permute-start | bytes 1572872 | tf_op jit(solution)/shard_map/ppermute | solution.py:18
  58.7 1.1 constant_dynamic-update-slice_fusion.4
  59.8 1.2 constant_dynamic-update-slice_fusion.1
  61.0 0.2 constant_dynamic-update-slice_fusion
  61.3 2.1 %fusion.64 = (f32[16,4,32]{2,1,0:T(4,128)S(1)}, f32[16,4,32,160]{3,2,1,0:T(8,128)S(1)}) fusion(bf16[32,16,4,128]{3,2,1,0:T(4,128)(2,1)S(1)} %bitcast.96, bf16[160,16,4,128]{3,1,0,2:T(8,128)(2,1)S(1)} %bitcast.93, pred[32,160]{1,0:T(8,128)(4,1)S(1)} %fusion.56), kind=kOutput, calls=%fused_computation.90 | convolution fusion | flops 84867072 | bytes 4469760 | tf_op jit(solution)/shard_map/qrhd,krhd->rhqk/dot_general | solution.py:51
  63.4 0.7 fusion.17
  64.2 0.6 fusion.65
  64.8 1.3 copy-done.4
  66.2 0.3 fusion.15
  66.8 0.1 copy.68
  66.9 0.2 stack_reshape.19
  67.1 0.2 stack.13
  67.3 1.9 %constant_dynamic-update-slice_fusion.11 = bf16[2560,4,128]{0,2,1:T(8,128)(2,1)} fusion(bf16[512,4,128]{0,2,1:T(8,128)(2,1)} %collective-permute-done.5), kind=kLoop, calls=%fused_computation.71 | loop fusion | bytes 1048576
  69.2 1.9 %constant_dynamic-update-slice_fusion.10 = bf16[2560,4,128]{0,2,1:T(8,128)(2,1)} fusion(bf16[2560,4,128]{0,2,1:T(8,128)(2,1)} %constant_dynamic-update-slice_fusion.11, bf16[512,4,128]{0,2,1:T(8,128)(2,1)} %collective-permute-done.6), kind=kLoop, calls=%fused_computation.70 | loop fusion | bytes 1048576
  71.1 10.5 %collective-permute-done.7 = bf16[512,4,128]{0,2,1:T(8,128)(2,1)} collective-permute-done((bf16[512,4,128]{0,2,1:T(8,128)(2,1)S(1)}, bf16[512,4,128]{0,2,1:T(8,128)(2,1)}, u32[]{:S(2)}, u32[]{:S(2)}) %collective-permute-start.7) | collective-permute-done | bytes 524320 | tf_op jit(solution)/shard_map/ppermute | solution.py:18
  81.6 1.9 %constant_dynamic-update-slice_fusion.9 = bf16[2560,4,128]{0,2,1:T(8,128)(2,1)} fusion(bf16[2560,4,128]{0,2,1:T(8,128)(2,1)} %constant_dynamic-update-slice_fusion.10, bf16[512,4,128]{0,2,1:T(8,128)(2,1)} %collective-permute-done.7), kind=kLoop, calls=%fused_computation.69 | loop fusion | bytes 1048576
  83.5 17.7 %collective-permute-done.4 = bf16[512,4,128]{0,2,1:T(8,128)(2,1)} collective-permute-done((bf16[512,4,128]{0,2,1:T(8,128)(2,1)S(1)}, bf16[512,4,128]{0,2,1:T(8,128)(2,1)}, u32[]{:S(2)}, u32[]{:S(2)}) %collective-permute-start.4) | collective-permute-done | bytes 524320 | tf_op jit(solution)/shard_map/ppermute | solution.py:18
  101.1 2.0 %constant_dynamic-update-slice_fusion.8 = bf16[2560,4,128]{0,2,1:T(8,128)(2,1)} fusion(bf16[2560,4,128]{0,2,1:T(8,128)(2,1)} %constant_dynamic-update-slice_fusion.9, bf16[512,4,128]{0,2,1:T(8,128)(2,1)} %collective-permute-done.4), kind=kLoop, calls=%fused_computation.68 | loop fusion | bytes 1048576
  103.1 0.9 constant_dynamic-update-slice_fusion.7
  104.0 4.4 %copy.89 = bf16[2560,4,128]{2,0,1:T(8,128)(2,1)} copy(bf16[2560,4,128]{0,2,1:T(8,128)(2,1)} %constant_dynamic-update-slice_fusion.7) | data formatting | bytes 5242880 | tf_op jit(solution)/shard_map/concatenate | solution.py:91
  108.4 4.3 %fusion.31 = f32[32,16,4,128]{3,0,2,1:T(8,128)S(1)} fusion(bf16[160,16,4,128]{3,1,0,2:T(8,128)(2,1)} %bitcast.88, f32[16,4,32,160]{3,2,1,0:T(8,128)} %copy-done.5, f32[16,4,32]{2,1,0:T(4,128)S(1)} %get-tuple-element.9, f32[32,16,4]{0,2,1:T(4,128)S(1)} %bitcast.92), kind=kOutput, calls=%fused_computation.34 | convolution fusion | flops 84803584 | bytes 4997120 | tf_op jit(solution)/shard_map/rhqk,krhd->qrhd/dot_general | solution.py:66
  112.7 1.6 %copy.91 = f32[32,16,4,128]{3,1,0,2:T(8,128)} copy(f32[32,16,4,128]{3,0,2,1:T(8,128)S(1)} %fusion.31) | data formatting | bytes 2097152 | tf_op jit(solution)/shard_map/div | solution.py:72
  114.3 2.5 %copy.93 = f32[1,512,4,128]{1,3,2,0:T(8,128)} copy(f32[1,512,4,128]{3,1,2,0:T(8,128)} %bitcast.85) | data formatting | bytes 2097152 | tf_op jit(solution)/shard_map/stack;reshape | solution.py:107
  116.8 2.2 %pad_maximum_fusion = bf16[1024,4,128]{0,2,1:T(8,128)(2,1)} fusion(bf16[512,4,128]{0,2,1:T(8,128)(2,1)S(1)} %copy.78, bf16[512,4,128]{0,2,1:T(8,128)(2,1)} %collective-permute-done.4), kind=kLoop, calls=%fused_computation.36 | loop fusion | flops 2097152 | bytes 2097152 | tf_op jit(solution)/shard_map/concatenate | solution.py:91
  119.0 2.3 %copy.81 = bf16[1024,4,128]{2,0,1:T(8,128)(2,1)} copy(bf16[1024,4,128]{0,2,1:T(8,128)(2,1)} %pad_maximum_fusion) | data formatting | bytes 2097152 | tf_op jit(solution)/shard_map/concatenate | solution.py:91
  121.3 2.6 %fusion.26 = f32[128,4,4,128]{3,0,2,1:T(8,128)S(1)} fusion(f32[4,4,128,256]{2,3,1,0:T(8,128)} %copy-done.4, bf16[256,4,4,128]{3,1,0,2:T(4,128)(2,1)} %bitcast.90, f32[4,4,128]{2,1,0:T(4,128)S(1)} %get-tuple-element.11, f32[128,4,4]{0,2,1:T(4,128)S(1)} %bitcast.95), kind=kOutput, calls=%fused_computation.28 | convolution fusion | flops 135528448 | bytes 4210688 | tf_op jit(solution)/shard_map/rhqk,krhd->qrhd/dot_general | solution.py:66
  123.9 1.6 %copy.84 = f32[128,4,4,128]{3,1,0,2:T(4,128)} copy(f32[128,4,4,128]{3,0,2,1:T(8,128)S(1)} %fusion.26) | data formatting | bytes 2097152 | tf_op jit(solution)/shard_map/div | solution.py:72
  125.6 2.6 %copy.92 = f32[1,512,4,128]{1,3,2,0:T(8,128)} copy(f32[1,512,4,128]{3,1,2,0:T(8,128)} %bitcast.86) | data formatting | bytes 2097152 | tf_op jit(solution)/shard_map/stack;reshape | solution.py:107
  128.2 2.3 %fusion.2 = (f32[4,512]{1,0:T(4,128)S(1)}, f32[4,640,512]{2,1,0:T(8,128)S(1)}) fusion(pred[512,640]{0,1:T(8,128)(4,1)S(1)} %fusion.30, bf16[512,4,128]{2,1,0:T(4,128)(2,1)} %param.4, bf16[1024,4,128]{2,0,1:T(8,128)(2,1)} %copy-done.6), kind=kOutput, calls=%fused_computation.4 | convolution fusion | flops 339474432 | bytes 6758400 | tf_op jit(solution)/shard_map/qrhd,krhd->rhqk/dot_general | solution.py:51
  130.5 1.1 fusion.1
  131.7 2.7 %divide_bitcast_fusion = f32[1,512,4,128]{1,3,2,0:T(8,128)S(1)} fusion(f32[4,640,512]{2,1,0:T(8,128)S(1)} %get-tuple-element.14, f32[4,512]{1,0:T(4,128)S(1)} %get-tuple-element.13, pred[512,640]{0,1:T(8,128)(4,1)S(1)} %fusion.30, bf16[512,4,128]{0,2,1:T(8,128)(2,1)} %collective-permute-done.4, bf16[512,4,128]{0,2,1:T(8,128)(2,1)S(1)} %copy.78, ...), kind=kOutput, calls=%fused_computation.40 | convolution fusion | flops 342360064 | bytes 7684096 | tf_op jit(solution)/shard_map/rhqk,krhd->qrhd/dot_general | solution.py:66
  134.4 0.4 fusion.3
  134.9 5.7 %all_to_all.5 = bf16[2,512,512]{1,2,0:T(8,128)(2,1)S(1)} all-to-all(bf16[2,512,512]{1,2,0:T(8,128)(2,1)S(1)} %broadcast_in_dim.75), channel_id=1, replica_groups=mesh['sp'=256,'tp'=2] {'tp'}, dimensions={0} | all-to-all | bytes 2097152 | tf_op jit(solution)/shard_map/all_to_all | solution.py:23
  140.6 2.3 %convolution_convert_fusion = bf16[512,1024]{1,0:T(8,128)(2,1)} fusion(bf16[512,1024]{0,1:T(8,128)(2,1)S(1)} %bitcast.87, bf16[1024,1024]{1,0:T(8,128)(2,1)S(1)} %copy-done), kind=kOutput, calls=%fused_computation.24 | convolution fusion | flops 1074266112 | bytes 4194304 | tf_op jit(solution)/shard_map/dot_general | solution.py:110
  (37 shorter events, 0.7 us)
Async XLA Ops:
  0.0 140.6 %copy-start = (bf16[1024,1024]{1,0:T(8,128)(2,1)S(1)}, bf16[1024,1024]{1,0:T(8,128)(2,1)}, u32[]{:S(2)}) copy-start(bf16[1024,1024]{1,0:T(8,128)(2,1)} %param.7) | copy-start | bytes 6291460
  2.1 57.7 %collective-permute-start = (bf16[512,4,128]{2,0,1:T(8,128)(2,1)}, bf16[512,4,128]{2,0,1:T(8,128)(2,1)}, u32[]{:S(2)}, u32[]{:S(2)}) collective-permute-start(bf16[512,4,128]{2,0,1:T(8,128)(2,1)} %copy.63), channel_id=1, source_target_pairs={{0,2},{2,4},{4,6},{6,8},{8,10},{10,12},{12,14},{14,16},{16,18},{18... | collective-permute-start | bytes 1572872 | tf_op jit(solution)/shard_map/ppermute | solution.py:18
  5.2 18.1 %collective-permute-start.1 = (bf16[512,4,128]{2,0,1:T(8,128)(2,1)}, bf16[512,4,128]{2,0,1:T(8,128)(2,1)}, u32[]{:S(2)}, u32[]{:S(2)}) collective-permute-start(bf16[512,4,128]{2,0,1:T(8,128)(2,1)} %copy.63), channel_id=1, source_target_pairs={{0,8},{2,10},{4,12},{6,14},{8,16},{10,18},{12,20},{14,22},{16,24},... | collective-permute-start | bytes 1572872 | tf_op jit(solution)/shard_map/ppermute | solution.py:18
  8.4 28.6 %collective-permute-start.2 = (bf16[512,4,128]{2,0,1:T(8,128)(2,1)}, bf16[512,4,128]{2,0,1:T(8,128)(2,1)}, u32[]{:S(2)}, u32[]{:S(2)}) collective-permute-start(bf16[512,4,128]{2,0,1:T(8,128)(2,1)} %copy.63), channel_id=1, source_target_pairs={{0,6},{2,8},{4,10},{6,12},{8,14},{10,16},{12,18},{14,20},{16,22},{... | collective-permute-start | bytes 1572872 | tf_op jit(solution)/shard_map/ppermute | solution.py:18
  12.8 36.4 %collective-permute-start.3 = (bf16[512,4,128]{2,0,1:T(8,128)(2,1)}, bf16[512,4,128]{2,0,1:T(8,128)(2,1)}, u32[]{:S(2)}, u32[]{:S(2)}) collective-permute-start(bf16[512,4,128]{2,0,1:T(8,128)(2,1)} %copy.63), channel_id=1, source_target_pairs={{0,4},{2,6},{4,8},{6,10},{8,12},{10,14},{12,16},{14,18},{16,20},{1... | collective-permute-start | bytes 1572872 | tf_op jit(solution)/shard_map/ppermute | solution.py:18
  17.6 43.5 %copy-start.3 = (bf16[512,4,128]{2,1,0:T(4,128)(2,1)S(1)}, bf16[512,4,128]{2,1,0:T(4,128)(2,1)}, u32[]{:S(2)}) copy-start(bf16[512,4,128]{2,1,0:T(4,128)(2,1)} %param.5) | copy-start | bytes 1572868
  17.6 49.7 %collective-permute-start.5 = (bf16[512,4,128]{0,2,1:T(8,128)(2,1)S(1)}, bf16[512,4,128]{0,2,1:T(8,128)(2,1)}, u32[]{:S(2)}, u32[]{:S(2)}) collective-permute-start(bf16[512,4,128]{0,2,1:T(8,128)(2,1)S(1)} %copy.78), channel_id=1, source_target_pairs={{0,8},{2,10},{4,12},{6,14},{8,16},{10,18},{12,20},{14,22},{16,24},... | collective-permute-start | bytes 1572872 | tf_op jit(solution)/shard_map/ppermute | solution.py:18
  23.2 46.0 %collective-permute-start.6 = (bf16[512,4,128]{0,2,1:T(8,128)(2,1)S(1)}, bf16[512,4,128]{0,2,1:T(8,128)(2,1)}, u32[]{:S(2)}, u32[]{:S(2)}) collective-permute-start(bf16[512,4,128]{0,2,1:T(8,128)(2,1)S(1)} %copy.78), channel_id=1, source_target_pairs={{0,6},{2,8},{4,10},{6,12},{8,14},{10,16},{12,18},{14,20},{16,22},{... | collective-permute-start | bytes 1572872 | tf_op jit(solution)/shard_map/ppermute | solution.py:18
  37.0 24.3 %copy-start.7 = (bf16[512,4,128]{2,1,0:T(4,128)(2,1)S(1)}, bf16[512,4,128]{2,1,0:T(4,128)(2,1)}, u32[]{:S(2)}) copy-start(bf16[512,4,128]{2,1,0:T(4,128)(2,1)} %param.4) | copy-start | bytes 1572868
  37.0 44.6 %collective-permute-start.7 = (bf16[512,4,128]{0,2,1:T(8,128)(2,1)S(1)}, bf16[512,4,128]{0,2,1:T(8,128)(2,1)}, u32[]{:S(2)}, u32[]{:S(2)}) collective-permute-start(bf16[512,4,128]{0,2,1:T(8,128)(2,1)S(1)} %copy.78), channel_id=1, source_target_pairs={{0,4},{2,6},{4,8},{6,10},{8,12},{10,14},{12,16},{14,18},{16,20},{1... | collective-permute-start | bytes 1572872 | tf_op jit(solution)/shard_map/ppermute | solution.py:18
  49.2 52.0 %collective-permute-start.4 = (bf16[512,4,128]{0,2,1:T(8,128)(2,1)S(1)}, bf16[512,4,128]{0,2,1:T(8,128)(2,1)}, u32[]{:S(2)}, u32[]{:S(2)}) collective-permute-start(bf16[512,4,128]{0,2,1:T(8,128)(2,1)S(1)} %copy.78), channel_id=1, source_target_pairs={{0,2},{2,4},{4,6},{6,8},{8,10},{10,12},{12,14},{14,16},{16,18},{18... | collective-permute-start | bytes 1572872 | tf_op jit(solution)/shard_map/ppermute | solution.py:18
  61.3 2.9 %copy-start.6 = (bf16[1024,4,128]{2,0,1:T(8,128)(2,1)}, bf16[1024,4,128]{2,0,1:T(8,128)(2,1)S(1)}, u32[]{:S(2)}) copy-start(bf16[1024,4,128]{2,0,1:T(8,128)(2,1)S(1)} %get-tuple-element.5) | copy-start | bytes 3145732
  63.4 1.4 copy-start.5
  64.8 1.4 copy-start.4
  131.7 2.7 %copy-start.1 = (f32[1,512,4,128]{1,3,2,0:T(8,128)S(1)}, f32[1,512,4,128]{1,3,2,0:T(8,128)}, u32[]{:S(2)}) copy-start(f32[1,512,4,128]{1,3,2,0:T(8,128)} %copy.93) | copy-start | bytes 3145732
  131.7 2.7 %copy-start.2 = (f32[1,512,4,128]{1,3,2,0:T(8,128)S(1)}, f32[1,512,4,128]{1,3,2,0:T(8,128)}, u32[]{:S(2)}) copy-start(f32[1,512,4,128]{1,3,2,0:T(8,128)} %copy.92) | copy-start | bytes 3145732
where the time goes:
time: 144 us; the launch traced here: 143 us
  starting transfers between devices  50.7 us (35%)
  local copies, waits for them, and re-layouts  34.1 us (24%)
  waiting for transfers between devices  29.8 us (21%)
  matrix products  16.8 us (12%)
  blocking collectives  5.73 us (4%)
  other arithmetic  5.42 us (4%)
    ppermute x8, starting transfers between devices, from_behind(): return lax.ppermute(block, axis, route)  50.7 us
    ppermute x8, waiting for transfers between devices, from_behind(): return lax.ppermute(block, axis, route)  29.8 us
    unnamed x26, local copies, waits for them, and re-layouts  17 us
    dot_general x3, matrix products, branch_attend(): jnp.einsum('rhqk,krhd->qrhd', numerators.astype(jnp.bfloat16), value_res,...  9.54 us
    concatenate x3, local copies, waits for them, and re-layouts, local(): value_holder = jnp.concatenate(earlier_values + [values], axis=0)  7.62 us
    all_to_all x1, blocking collectives, sent_to_all(): lax.all_to_all(jnp.broadcast_to(array[None], (peers, *array.shape)), axis...  5.73 us
    another operation x2, local copies, waits for them, and re-layouts, local(): jnp.stack([first_out, second_output, third_output])  5.16 us
    dot_general x3, matrix products, branch_attend(): jnp.einsum('qrhd,krhd->rhqk', query_res, key_res, preferred_element_type=...  4.95 us
  transfers between devices with their start and end apart: 8, of which 3 were waited for; matrix products, arithmetic and copies ran while one was open for 12% of the time, Pallas kernels for 0%

commit v1 on v0

v1 whole, which is shorter than its diff:
```python
import math

import jax
import jax.numpy as jnp
from jax import lax
from jax.experimental import pallas as pl
from jax.experimental.pallas import tpu as pltpu
from jax.sharding import Mesh
from jax.sharding import PartitionSpec as P

DILATION_TWO = 4
DILATION_THREE = 16
HEAD_DIM = 128
ROW_CHIPS = 4
BLOCK = 512
STEPS = BLOCK // DILATION_THREE
TILE = 128
SCALE = math.log2(math.e) / math.sqrt(HEAD_DIM)
LOWEST = -1e30
VMEM = pl.BlockSpec(memory_space=pltpu.VMEM)
SMEM = pl.BlockSpec(memory_space=pltpu.SMEM)


def pack_kernel(*refs):
    count = len(refs) // 2
    wide = refs[-1]
    for in_ref, out_ref in zip(refs[:count], refs[count : 2 * count]):
        wide[...] = in_ref[...].astype(jnp.float32)
        for head in range(4):
            for res in range(DILATION_THREE):
                rows = wide[pl.ds(4 * res + head, STEPS, stride=4 * DILATION_THREE), :]
                out_ref[head, res * STEPS : (res + 1) * STEPS, :] = rows.astype(jnp.bfloat16)


def pack(*arrays):
    shape = jax.ShapeDtypeStruct((4, BLOCK, HEAD_DIM), jnp.bfloat16)
    return pl.pallas_call(
        pack_kernel,
        out_shape=[shape] * len(arrays),
        in_specs=[VMEM] * len(arrays),
        out_specs=[VMEM] * len(arrays),
        scratch_shapes=[pltpu.VMEM((4 * BLOCK, HEAD_DIM), jnp.float32)],
        cost_estimate=pl.CostEstimate(
            flops=1000000, bytes_accessed=2 * 524288 * len(arrays), transcendentals=0
        ),
    )(*[array.reshape(4 * BLOCK, HEAD_DIM) for array in arrays])


def masks(order):
    q = lax.broadcasted_iota(jnp.int32, (TILE, TILE), 0)
    k = lax.broadcasted_iota(jnp.int32, (TILE, TILE), 1)
    return order(k) >= order(q), order(k) <= order(q)


def order_one(row):
    return (row % 8) * 16 + row // 8


def order_two(row):
    return (row % 32) * 4 + row // 32


def order_three(row):
    return row


def attend_tile(query, key, value, before, own):
    scores = lax.dot_general(
        query, key, (((1,), (1,)), ((), ())), preferred_element_type=jnp.float32
    )
    early = jnp.where(before, scores[:, :TILE], LOWEST)
    late = jnp.where(own, scores[:, TILE:], LOWEST)
    peak = jnp.max(jnp.maximum(early, late), axis=-1, keepdims=True)
    return early, late, peak, jnp.concatenate([value, jnp.ones_like(value)], axis=1)


def weigh(early, late, top, value):
    shares = jnp.concatenate(
        [jnp.exp2((early - top) * SCALE), jnp.exp2((late - top) * SCALE)], axis=1
    ).astype(jnp.bfloat16)
    both = jnp.dot(shares, value, preferred_element_type=jnp.float32)
    return both[:, :HEAD_DIM], both[:, HEAD_DIM:]


def attention_kernel(
    flag, q, k, v, k_back, v_back, out, top, total, acc, q_wide, k_wide, v_wide, natural
):
    has_back = flag[0] > 0

    for x in range(ROW_CHIPS):
        for res in range(DILATION_THREE):
            spot = (x, res // 4, res % 4)
            for source, target, shift in ((q, q_wide, 0), (k, k_wide, 1), (v, v_wide, 1)):
                rows = source[spot].astype(jnp.float32).reshape(4, 8, HEAD_DIM)
                target[4 * x + shift : 4 * x + shift + 4, res * 8 : res * 8 + 8, :] = rows
    for res in range(DILATION_THREE):
        for source, target in ((k_back, k_wide), (v_back, v_wide)):
            rows = source[3, res // 4, res % 4].astype(jnp.float32)
            target[0, res * 8 : res * 8 + 8, :] = rows[24:32]

    before, own = masks(order_one)

    def one(block, carry):
        x = block // 4
        j = pl.multiple_of((block % 4) * 8, 8)
        query = q_wide[block].astype(jnp.bfloat16)
        key = k_wide[pl.ds(block, 2)].reshape(2 * TILE, HEAD_DIM).astype(jnp.bfloat16)
        value = v_wide[pl.ds(block, 2)].reshape(2 * TILE, HEAD_DIM).astype(jnp.bfloat16)
        seen = before & ((block > 0) | has_back)
        early, late, peak, value = attend_tile(query, key, value, seen, own)
        high = jnp.broadcast_to(peak, (TILE, TILE))
        part, count = weigh(early, late, high, value)
        shape = (4, 4, 8, TILE)
        top[x, :, :, pl.ds(j, 8), :] = high.reshape(shape)
        total[x, :, :, pl.ds(j, 8), :] = count.reshape(shape)
        acc[x, :, :, pl.ds(j, 8), :] = part.reshape(shape)
        return carry

    lax.fori_loop(0, 16, one, 0)

    before, own = masks(order_two)
    for x in range(ROW_CHIPS):

        def two(res, carry, x=x):
            def rows(ref, index):
                return ref[index, :, res].reshape(TILE, HEAD_DIM)

            query = rows(q, x)
            if x == 0:
                key = jnp.concatenate([rows(k_back, 3), rows(k, 0)], axis=0)
                value = jnp.concatenate([rows(v_back, 3), rows(v, 0)], axis=0)
                seen = before & has_back
            else:
                key = jnp.concatenate([rows(k, x - 1), rows(k, x)], axis=0)
                value = jnp.concatenate([rows(v, x - 1), rows(v, x)], axis=0)
                seen = before
            early, late, peak, value = attend_tile(query, key, value, seen, own)
            old = rows(top, x)
            high = jnp.maximum(old, peak)
            part, count = weigh(early, late, high, value)
            fade = jnp.exp2((old - high) * SCALE)
            shape = (4, STEPS, TILE)
            total[x, :, res] = (rows(total, x) * fade + count).reshape(shape)
            acc[x, :, res] = (rows(acc, x) * fade + part).reshape(shape)
            top[x, :, res] = high.reshape(shape)
            return carry

        lax.fori_loop(0, DILATION_TWO, two, 0)

    before, own = masks(order_three)
    before = before & has_back

    def three(res, carry):
        def rows(ref):
            return ref[:, res // 4, res % 4].reshape(TILE, HEAD_DIM)

        key = jnp.concatenate([rows(k_back), rows(k)], axis=0)
        value = jnp.concatenate([rows(v_back), rows(v)], axis=0)
        early, late, peak, value = attend_tile(rows(q), key, value, before, own)
        old = rows(top)
        high = jnp.maximum(old, peak)
        part, count = weigh(early, late, high, value)
        fade = jnp.exp2((old - high) * SCALE)
        result = (rows(acc) * fade + part) / (rows(total) * fade + count)
        for x in range(ROW_CHIPS):
            natural[pl.ds(x * BLOCK + res, STEPS, stride=DILATION_THREE), :] = result[
                x * STEPS : (x + 1) * STEPS
            ]
        return carry

    lax.fori_loop(0, DILATION_THREE, three, 0)
    out[...] = natural[...].astype(jnp.bfloat16)


def attention(flag, q, k, v, k_back, v_back):
    split = (ROW_CHIPS, 4, 4, STEPS, HEAD_DIM)
    wide = (16, TILE, HEAD_DIM)
    return pl.pallas_call(
        attention_kernel,
        out_shape=jax.ShapeDtypeStruct((ROW_CHIPS * BLOCK, HEAD_DIM), jnp.bfloat16),
        in_specs=[SMEM] + [VMEM] * 5,
        out_specs=VMEM,
        scratch_shapes=[
            pltpu.VMEM(split, jnp.float32),
            pltpu.VMEM(split, jnp.float32),
            pltpu.VMEM(split, jnp.float32),
            pltpu.VMEM(wide, jnp.float32),
            pltpu.VMEM((17, TILE, HEAD_DIM), jnp.float32),
            pltpu.VMEM((17, TILE, HEAD_DIM), jnp.float32),
            pltpu.VMEM((ROW_CHIPS * BLOCK, HEAD_DIM), jnp.float32),
        ],
        cost_estimate=pl.CostEstimate(
            flops=2000000000, bytes_accessed=3000000, transcendentals=1600000
        ),
    )(flag, *[array.reshape(split) for array in (q, k, v, k_back, v_back)])


def first_half_kernel(place, mine, w, out):
    rows = pl.multiple_of(place[0] * BLOCK, BLOCK)
    features = jnp.concatenate([mine[head] for head in range(4)], axis=1)
    out[...] = jnp.dot(features, w[pl.ds(rows, BLOCK), :], preferred_element_type=jnp.float32)


def second_half_kernel(place, other, w, half, out):
    rows = pl.multiple_of((1 - place[0]) * BLOCK, BLOCK)
    features = jnp.concatenate([other[head] for head in range(4)], axis=1)
    product = jnp.dot(features, w[pl.ds(rows, BLOCK), :], preferred_element_type=jnp.float32)
    out[...] = (product + half[...]).astype(jnp.bfloat16)


def local(queries, keys, values, w_out):
    row = lax.axis_index("row")
    core = lax.axis_index("tp")
    rows = lax.axis_size("row")
    onward = [(i, i + 1) for i in range(rows - 1)]
    columns = w_out.shape[1]
    projection = pl.CostEstimate(
        flops=2 * BLOCK * BLOCK * columns, bytes_accessed=3000000, transcendentals=0
    )

    def across(array):
        return lax.all_to_all(array, "x", 0, 0, tiled=True)

    (k_pack,) = pack(keys)
    k = across(k_pack)
    k_back = lax.ppermute(k, "row", onward)
    v_pack, q_pack = pack(values, queries)
    v = across(v_pack)
    v_back = lax.ppermute(v, "row", onward)
    q = across(q_pack)
    flag = jnp.reshape(row, (1,)).astype(jnp.int32)
    attended = attention(flag, q, k, v, k_back, v_back)
    mine = across(attended.reshape(ROW_CHIPS, BLOCK, HEAD_DIM))
    other = lax.ppermute(mine, "tp", [(0, 1), (1, 0)])
    place = jnp.reshape(core, (1,)).astype(jnp.int32)
    half = pl.pallas_call(
        first_half_kernel,
        out_shape=jax.ShapeDtypeStruct((BLOCK, columns), jnp.float32),
        in_specs=[SMEM, VMEM, VMEM],
        out_specs=VMEM,
        cost_estimate=projection,
    )(place, mine, w_out)
    return pl.pallas_call(
        second_half_kernel,
        out_shape=jax.ShapeDtypeStruct((BLOCK, columns), jnp.bfloat16),
        in_specs=[SMEM, VMEM, VMEM, VMEM],
        out_specs=VMEM,
        cost_estimate=projection,
    )(place, other, w_out, half)


def solution(mesh):
    rows = mesh.shape["sp"] // ROW_CHIPS
    grid = Mesh(mesh.devices.reshape(rows, ROW_CHIPS, mesh.shape["tp"]), ("row", "x", "tp"))
    whole = ("row", "x")
    in_specs = (P(whole, "tp", None),) * 3 + (P(None, "tp"),)
    return jax.shard_map(
        local, mesh=grid, in_specs=in_specs, out_specs=P(whole, "tp"), check_vma=False
    )
```

time: 144 us -> 95.3 us (0.66)
  Pallas kernels: 0 us -> 35.3 us
  local copies, waits for them, and re-layouts: 34.1 us -> 1.64 us
  starting transfers between devices: 50.7 us -> 23.9 us
  matrix products: 16.8 us -> 0 us
  waiting for transfers between devices: 29.8 us -> 22.9 us
  other arithmetic: 5.42 us -> 0 us
  blocking collectives: 5.73 us -> 10.8 us
    ppermute x8 -> x3, starting transfers between devices: 50.7 us -> 13 us  [the longest x1 6.57 us: local(): other = lax.ppermute(mine, 'tp', [(0, 1), (1, 0)])]
    pallas_call x0 -> x5, Pallas kernels: none -> 35.3 us  [the longest x1 21.7 us: attention(): pl.pallas_call(attention_kernel, out_shape=jax.ShapeDtypeStruct((ROW_CHIP...]
    ppermute x8 -> x3, waiting for transfers between devices: 29.8 us -> 6.8 us  [the longest x1 6.79 us: local(): v_back = lax.ppermute(v, 'row', onward)]
    dot_general x7 -> x0, matrix products: 16.8 us -> none  [the longest x3 9.54 us: branch_attend(): jnp.einsum('rhqk,krhd->qrhd', numerators.astype(jnp.bfloat16), value_res,...]
    all_to_all x0 -> x3, waiting for transfers between devices: none -> 16.1 us  [across(): return lax.all_to_all(array, 'x', 0, 0, tiled=True)]
    unnamed x26 -> x14, local copies, waits for them, and re-layouts: 17 us -> 1.64 us
    all_to_all x0 -> x3, starting transfers between devices: none -> 11 us  [across(): return lax.all_to_all(array, 'x', 0, 0, tiled=True)]
    concatenate x4 -> x0, local copies, waits for them, and re-layouts: 7.87 us -> none  [the longest x3 7.62 us: local(): value_holder = jnp.concatenate(earlier_values + [values], axis=0)]
  transfers between devices with their start and end apart: 8 -> 6, of which waited for: 3 -> 4; matrix products, arithmetic and copies ran while one was open for 12% -> 0% of each run, Pallas kernels for 0% -> 7%
where the time goes in v1:
time: 95.3 us; the launch traced here: 94.8 us
  Pallas kernels  35.3 us (37%)
  starting transfers between devices  23.9 us (25%)
  waiting for transfers between devices  22.9 us (24%)
  blocking collectives  10.8 us (11%)
  local copies, waits for them, and re-layouts  1.64 us (2%)
    pallas_call x1, Pallas kernels, attention(): pl.pallas_call(attention_kernel, out_shape=jax.ShapeDtypeStruct((ROW_CHIP...  21.7 us
    all_to_all x3, waiting for transfers between devices, across(): return lax.all_to_all(array, 'x', 0, 0, tiled=True)  16.1 us
    all_to_all x3, starting transfers between devices, across(): return lax.all_to_all(array, 'x', 0, 0, tiled=True)  11 us
    all_to_all x1, blocking collectives, across(): return lax.all_to_all(array, 'x', 0, 0, tiled=True)  10.8 us
    ppermute x1, waiting for transfers between devices, local(): v_back = lax.ppermute(v, 'row', onward)  6.79 us
    ppermute x1, starting transfers between devices, local(): other = lax.ppermute(mine, 'tp', [(0, 1), (1, 0)])  6.57 us
    pallas_call x2, Pallas kernels, pack(): pl.pallas_call(pack_kernel, out_shape=[shape] * len(arrays), in_specs=[VM...  5.77 us
    pallas_call x1, Pallas kernels, local(): pl.pallas_call(second_half_kernel, out_shape=jax.ShapeDtypeStruct((BLOCK,...  4.06 us
  transfers between devices with their start and end apart: 6, of which 4 were waited for; matrix products, arithmetic and copies ran while one was open for 0% of the time, Pallas kernels for 7%

profile of v1, /device:TPU:257, one launch (start us, length us, event | category | flops | bytes accessed | tf_op | source)
XLA Modules:
  0.0 94.8 jit_solution(14051335859028100194)
XLA Ops:
  0.0 2.5 %shard_map.47 = bf16[4,512,128]{2,1,0:T(8,128)(2,1)} custom-call(bf16[2048,128]{1,0:T(8,128)(2,1)} %bitcast.11), custom_call_target="tpu_custom_call" | custom-call | flops 1000000 | bytes 1048576 | tf_op jit(solution)/shard_map/pallas_call | solution.py:37
  2.5 4.0 %all-to-all-start.1 = ((bf16[4,512,128]{2,1,0:T(8,128)(2,1)}), bf16[4,512,128]{2,1,0:T(8,128)(2,1)S(1)}, u32[]{:S(2)}, u32[]{:S(2)}) async-start(bf16[4,512,128]{2,1,0:T(8,128)(2,1)} %shard_map.47), calls=%async_computation.1 | async-start | bytes 1048576 | tf_op jit(solution)/shard_map/all_to_all | solution.py:222
  6.5 3.3 %shard_map.46 = (bf16[4,512,128]{2,1,0:T(8,128)(2,1)}, bf16[4,512,128]{2,1,0:T(8,128)(2,1)}) custom-call(bf16[2048,128]{1,0:T(8,128)(2,1)} %bitcast.12, bf16[2048,128]{1,0:T(8,128)(2,1)} %bitcast.13), custom_call_target="tpu_custom_call" | custom-call | flops 1000000 | bytes 2097152 | tf_op jit(solution)/shard_map/pallas_call | solution.py:37
  9.8 5.0 %all-to-all-done.1 = bf16[4,512,128]{2,1,0:T(8,128)(2,1)S(1)} async-done(((bf16[4,512,128]{2,1,0:T(8,128)(2,1)}), bf16[4,512,128]{2,1,0:T(8,128)(2,1)S(1)}, u32[]{:S(2)}, u32[]{:S(2)}) %all-to-all-start.1) | async-done | bytes 524320 | tf_op jit(solution)/shard_map/all_to_all | solution.py:222
  14.8 0.0 copy-start.2
  14.8 3.5 %all-to-all-start.2 = ((bf16[4,512,128]{2,1,0:T(8,128)(2,1)}), bf16[4,512,128]{2,1,0:T(8,128)(2,1)S(1)}, u32[]{:S(2)}, u32[]{:S(2)}) async-start(bf16[4,512,128]{2,1,0:T(8,128)(2,1)} %get-tuple-element.8), calls=%async_computation.2 | async-start | bytes 1048576 | tf_op jit(solution)/shard_map/all_to_all | solution.py:222
  18.3 3.2 %collective-permute-start = (bf16[4,512,128]{2,1,0:T(8,128)(2,1)S(1)}, bf16[4,512,128]{2,1,0:T(8,128)(2,1)S(1)}, u32[]{:S(2)}, u32[]{:S(2)}) collective-permute-start(bf16[4,512,128]{2,1,0:T(8,128)(2,1)S(1)} %all-to-all-done.1), channel_id=1, source_target_pairs={{0,8},{8,16},{16,24},{24,32},{32,40},{40,48},{48,56},{56,64},{64,7... | collective-permute-start | bytes 1572872 | tf_op jit(solution)/shard_map/ppermute | solution.py:226
  21.5 3.9 %all-to-all-done.2 = bf16[4,512,128]{2,1,0:T(8,128)(2,1)S(1)} async-done(((bf16[4,512,128]{2,1,0:T(8,128)(2,1)}), bf16[4,512,128]{2,1,0:T(8,128)(2,1)S(1)}, u32[]{:S(2)}, u32[]{:S(2)}) %all-to-all-start.2) | async-done | bytes 524320 | tf_op jit(solution)/shard_map/all_to_all | solution.py:222
  25.4 0.0 copy-start.3
  25.4 3.2 %collective-permute-start.1 = (bf16[4,512,128]{2,1,0:T(8,128)(2,1)S(1)}, bf16[4,512,128]{2,1,0:T(8,128)(2,1)S(1)}, u32[]{:S(2)}, u32[]{:S(2)}) collective-permute-start(bf16[4,512,128]{2,1,0:T(8,128)(2,1)S(1)} %all-to-all-done.2), channel_id=1, source_target_pairs={{0,8},{8,16},{16,24},{24,32},{32,40},{40,48},{48,56},{56,64},{64,7... | collective-permute-start | bytes 1572872 | tf_op jit(solution)/shard_map/ppermute | solution.py:229
  28.6 3.5 %all-to-all-start = ((bf16[4,512,128]{2,1,0:T(8,128)(2,1)}), bf16[4,512,128]{2,1,0:T(8,128)(2,1)S(1)}, u32[]{:S(2)}, u32[]{:S(2)}) async-start(bf16[4,512,128]{2,1,0:T(8,128)(2,1)} %get-tuple-element.7), calls=%async_computation | async-start | bytes 1048576 | tf_op jit(solution)/shard_map/all_to_all | solution.py:222
  32.1 7.2 %all-to-all-done = bf16[4,512,128]{2,1,0:T(8,128)(2,1)S(1)} async-done(((bf16[4,512,128]{2,1,0:T(8,128)(2,1)}), bf16[4,512,128]{2,1,0:T(8,128)(2,1)S(1)}, u32[]{:S(2)}, u32[]{:S(2)}) %all-to-all-start) | async-done | bytes 524320 | tf_op jit(solution)/shard_map/all_to_all | solution.py:222
  39.3 0.0 copy-start.4
  39.3 0.0 collective-permute-done
  39.3 0.0 copy-start.5
  39.3 6.8 %collective-permute-done.1 = bf16[4,512,128]{2,1,0:T(8,128)(2,1)S(1)} collective-permute-done((bf16[4,512,128]{2,1,0:T(8,128)(2,1)S(1)}, bf16[4,512,128]{2,1,0:T(8,128)(2,1)S(1)}, u32[]{:S(2)}, u32[]{:S(2)}) %collective-permute-start.1) | collective-permute-done | bytes 524320 | tf_op jit(solution)/shard_map/ppermute | solution.py:229
  46.1 0.0 copy-start.6
  46.1 0.0 copy-done.2
  46.1 0.0 copy-done.3
  46.1 0.0 copy-done.4
  46.1 0.0 copy-done.5
  46.1 0.8 copy-done.6
  47.0 21.7 %shard_map.48 = bf16[2048,128]{1,0:T(8,128)(2,1)} custom-call(s32[1]{0:T(128)} %bitcast.1.flag, bf16[4,4,4,32,128]{4,3,2,1,0:T(8,128)(2,1)} %bitcast.16, bf16[4,4,4,32,128]{4,3,2,1,0:T(8,128)(2,1)} %bitcast.14, bf16[4,4,4,32,128]{4,3,2,1,0:T(8,128)(2,1)} %bitcast.15, bf16[4,4,4,32,128]{4,3,2,1,0:T(8,128)(2,1)} %bitcast.18, bf16[4,4,4,32,128]{4,3,2,1,0:T(8,128)(2,1)} %bitcast.19), custom_call_target="tpu_custom_call" | custom-call | flops 2000000000 | bytes 3000000 | tf_op jit(solution)/shard_map/pallas_call | solution.py:178
  68.6 10.8 %all_to_all.20.mine = bf16[4,512,128]{2,1,0:T(8,128)(2,1)S(1)} all-to-all(bf16[4,512,128]{2,1,0:T(8,128)(2,1)} %bitcast.17), channel_id=1, replica_groups=mesh['row'=64,'x'=4,'tp'=2] {'x'}, dimensions={0} | all-to-all | bytes 1048576 | tf_op jit(solution)/shard_map/all_to_all | solution.py:222
  79.5 0.0 copy-start
  79.5 6.6 %collective-permute-start.2 = (bf16[4,512,128]{2,1,0:T(8,128)(2,1)S(1)}, bf16[4,512,128]{2,1,0:T(8,128)(2,1)S(1)}, u32[]{:S(2)}, u32[]{:S(2)}) collective-permute-start(bf16[4,512,128]{2,1,0:T(8,128)(2,1)S(1)} %all_to_all.20.mine), channel_id=1, source_target_pairs={{0,1},{1,0},{2,3},{3,2},{4,5},{5,4},{6,7},{7,6},{8,9},{9,8},{10,11... | collective-permute-start | bytes 1572872 | tf_op jit(solution)/shard_map/ppermute | solution.py:234
  86.0 0.0 copy-done
  86.1 3.8 %shard_map.49.half = f32[512,1024]{1,0:T(8,128)} custom-call(s32[1]{0:T(128)} %bitcast.place, bf16[4,512,128]{2,1,0:T(8,128)(2,1)} %copy-done, bf16[1024,1024]{1,0:T(8,128)(2,1)} %w.3), custom_call_target="tpu_custom_call" | custom-call | flops 536870912 | bytes 3000000 | tf_op jit(solution)/shard_map/pallas_call | solution.py:236
  89.9 0.0 collective-permute-done.2.other
  89.9 0.0 copy-start.1
  89.9 0.8 copy-done.1
  90.7 4.1 %shard_map.50 = bf16[512,1024]{1,0:T(8,128)(2,1)} custom-call(s32[1]{0:T(128)} %bitcast.place, bf16[4,512,128]{2,1,0:T(8,128)(2,1)} %copy-done.1, bf16[1024,1024]{1,0:T(8,128)(2,1)} %w.3, f32[512,1024]{1,0:T(8,128)} %shard_map.49.half), custom_call_target="tpu_custom_call" | custom-call | flops 536870912 | bytes 3000000 | tf_op jit(solution)/shard_map/pallas_call | solution.py:243
Async XLA Ops:
  2.5 12.3 %all-to-all-start.1 = ((bf16[4,512,128]{2,1,0:T(8,128)(2,1)}), bf16[4,512,128]{2,1,0:T(8,128)(2,1)S(1)}, u32[]{:S(2)}, u32[]{:S(2)}) async-start(bf16[4,512,128]{2,1,0:T(8,128)(2,1)} %shard_map.47), calls=%async_computation.1 | async-start | bytes 1048576 | tf_op jit(solution)/shard_map/all_to_all | solution.py:222
  14.8 31.3 %copy-start.2 = (bf16[4,512,128]{2,1,0:T(8,128)(2,1)}, bf16[4,512,128]{2,1,0:T(8,128)(2,1)S(1)}, u32[]{:S(2)}) copy-start(bf16[4,512,128]{2,1,0:T(8,128)(2,1)S(1)} %all-to-all-done.1) | copy-start | bytes 1572868
  14.8 10.6 %all-to-all-start.2 = ((bf16[4,512,128]{2,1,0:T(8,128)(2,1)}), bf16[4,512,128]{2,1,0:T(8,128)(2,1)S(1)}, u32[]{:S(2)}, u32[]{:S(2)}) async-start(bf16[4,512,128]{2,1,0:T(8,128)(2,1)} %get-tuple-element.8), calls=%async_computation.2 | async-start | bytes 1048576 | tf_op jit(solution)/shard_map/all_to_all | solution.py:222
  18.3 21.0 %collective-permute-start = (bf16[4,512,128]{2,1,0:T(8,128)(2,1)S(1)}, bf16[4,512,128]{2,1,0:T(8,128)(2,1)S(1)}, u32[]{:S(2)}, u32[]{:S(2)}) collective-permute-start(bf16[4,512,128]{2,1,0:T(8,128)(2,1)S(1)} %all-to-all-done.1), channel_id=1, source_target_pairs={{0,8},{8,16},{16,24},{24,32},{32,40},{40,48},{48,56},{56,64},{64,7... | collective-permute-start | bytes 1572872 | tf_op jit(solution)/shard_map/ppermute | solution.py:226
  25.4 20.7 %copy-start.3 = (bf16[4,512,128]{2,1,0:T(8,128)(2,1)}, bf16[4,512,128]{2,1,0:T(8,128)(2,1)S(1)}, u32[]{:S(2)}) copy-start(bf16[4,512,128]{2,1,0:T(8,128)(2,1)S(1)} %all-to-all-done.2) | copy-start | bytes 1572868
  25.4 20.7 %collective-permute-start.1 = (bf16[4,512,128]{2,1,0:T(8,128)(2,1)S(1)}, bf16[4,512,128]{2,1,0:T(8,128)(2,1)S(1)}, u32[]{:S(2)}, u32[]{:S(2)}) collective-permute-start(bf16[4,512,128]{2,1,0:T(8,128)(2,1)S(1)} %all-to-all-done.2), channel_id=1, source_target_pairs={{0,8},{8,16},{16,24},{24,32},{32,40},{40,48},{48,56},{56,64},{64,7... | collective-permute-start | bytes 1572872 | tf_op jit(solution)/shard_map/ppermute | solution.py:229
  28.6 10.7 %all-to-all-start = ((bf16[4,512,128]{2,1,0:T(8,128)(2,1)}), bf16[4,512,128]{2,1,0:T(8,128)(2,1)S(1)}, u32[]{:S(2)}, u32[]{:S(2)}) async-start(bf16[4,512,128]{2,1,0:T(8,128)(2,1)} %get-tuple-element.7), calls=%async_computation | async-start | bytes 1048576 | tf_op jit(solution)/shard_map/all_to_all | solution.py:222
  39.3 6.8 %copy-start.4 = (bf16[4,512,128]{2,1,0:T(8,128)(2,1)}, bf16[4,512,128]{2,1,0:T(8,128)(2,1)S(1)}, u32[]{:S(2)}) copy-start(bf16[4,512,128]{2,1,0:T(8,128)(2,1)S(1)} %all-to-all-done) | copy-start | bytes 1572868
  39.3 6.8 %copy-start.5 = (bf16[4,512,128]{2,1,0:T(8,128)(2,1)}, bf16[4,512,128]{2,1,0:T(8,128)(2,1)S(1)}, u32[]{:S(2)}) copy-start(bf16[4,512,128]{2,1,0:T(8,128)(2,1)S(1)} %collective-permute-done) | copy-start | bytes 1572868
  46.1 0.8 copy-start.6
  79.5 6.6 %copy-start = (bf16[4,512,128]{2,1,0:T(8,128)(2,1)}, bf16[4,512,128]{2,1,0:T(8,128)(2,1)S(1)}, u32[]{:S(2)}) copy-start(bf16[4,512,128]{2,1,0:T(8,128)(2,1)S(1)} %all_to_all.20.mine) | copy-start | bytes 1572868
  79.5 10.4 %collective-permute-start.2 = (bf16[4,512,128]{2,1,0:T(8,128)(2,1)S(1)}, bf16[4,512,128]{2,1,0:T(8,128)(2,1)S(1)}, u32[]{:S(2)}, u32[]{:S(2)}) collective-permute-start(bf16[4,512,128]{2,1,0:T(8,128)(2,1)S(1)} %all_to_all.20.mine), channel_id=1, source_target_pairs={{0,1},{1,0},{2,3},{3,2},{4,5},{5,4},{6,7},{7,6},{8,9},{9,8},{10,11... | collective-permute-start | bytes 1572872 | tf_op jit(solution)/shard_map/ppermute | solution.py:234
  89.9 0.8 copy-start.1
